TPU v7x, 32 devices: a whole 2x2x4 slice. The times are simulated.
32 devices in a mesh: sp: 4 (over y, x), tp: 8 (over z, core).
Axes of the slice: x: 2, y: 2, z: 4, core: 2. Of those that a mesh axis runs over, the one named last changes fastest.
Arguments:
- query_rows: bfloat16 [8192, 1024], P('sp', 'tp'), may hold values from -6 to 6
- key_rows: bfloat16 [8192, 1024], P('sp', 'tp'), may hold values from -6 to 6
- value_rows: bfloat16 [8192, 1024], P('sp', 'tp'), may hold values from -6 to 6
- gate_rows: bfloat16 [8192, 1024], P('sp', 'tp'), may hold values from -6 to 6
- log_decay: float32 [16, 8192], P('tp', 'sp'), may hold values from -1 to 0
- residual: bfloat16 [8192, 2048], P(('sp', 'tp')), may hold values from -6 to 6
- head_gain: float32 [1024], P('tp'), may hold values from 0.1 to 1.9
- out_weight: bfloat16 [1024, 2048], P(None, 'tp'), may hold values from -0.1875 to 0.1875
- norm_gain: float32 [2048], replicated, may hold values from 0.1 to 1.9
- expert_ids: int32 [8192, 2], P(('sp', 'tp')), may hold values from 0 to 3, all different within a row; in each aligned block of 256 rows (0 to 255, 256 to 511, ...) at most 192 rows name the same one
- route_weights: float32 [8192, 2], P(('sp', 'tp')), may hold values from 0.2 to 1
- expert_gate: bfloat16 [2048, 4096], P(None, ('sp', 'tp')), may hold values from -0.125 to 0.125
- expert_up: bfloat16 [2048, 4096], P(None, ('sp', 'tp')), may hold values from -0.125 to 0.125
- expert_down: bfloat16 [2048, 4096], P(None, ('sp', 'tp')), may hold values from -0.1875 to 0.1875
- shared_gate: bfloat16 [2048, 512], replicated, may hold values from -0.125 to 0.125
- shared_up: bfloat16 [2048, 512], replicated, may hold values from -0.125 to 0.125
- shared_down: bfloat16 [2048, 512], replicated, may hold values from -0.25 to 0.25
Outputs:
- result: bfloat16 [8192, 2048], P(('sp', 'tp'))
Inputs may be any that keep to these rules, and one draw needn't show every extreme that they name: `expert_ids`: each row names 2 different experts. Within the rows of one device (aligned blocks of 256 rows) no expert is named by more than 192 rows, and in some block an expert is named by exactly 192 rows.
All inputs are finite; a program needn't handle non-finite values.
Results may differ from a plain program's by a relative error of at most 0.0075.
Values may be sent and summed in bfloat16 or wider, within the bound.
A program may use at most 128 MiB of HBM per device.

v0:
```python
import jax
import jax.numpy as jnp
from jax import lax
from jax.sharding import PartitionSpec as P

HEAD = 64
SPAN = 512
eps = 1e-05


def entering(value, axis, join, neutral):
    count, mine = (lax.axis_size(axis), lax.axis_index(axis))
    pieces = jax.tree.map(lambda part: lax.all_gather(part, axis), value)
    so_far = jax.tree.map(
        lambda part, zero: jnp.full_like(part, 0) + jnp.asarray(zero, part.dtype), value, neutral
    )

    def hop(position, so_far):
        longer = join(so_far, jax.tree.map(lambda part: part[position], pieces))
        return jax.tree.map(lambda new, old: jnp.where(position < mine, new, old), longer, so_far)

    return lax.fori_loop(0, count - 1, hop, so_far)


def block_pass(queries, key_heads, values, log_decay, state):
    rows, heads, width = queries.shape
    count = rows // SPAN
    scale = width ** (-0.5)
    query_blocks = queries.reshape(count, SPAN, heads, width)
    key_blocks = key_heads.reshape(count, SPAN, heads, width)
    value_blocks = values.reshape(count, SPAN, heads, width)
    decay_blocks = log_decay.reshape(heads, count, SPAN).transpose(1, 0, 2)
    offsets = jnp.arange(SPAN, dtype=jnp.int32)
    causal = offsets[:, None] >= offsets[None, :]

    def advance(carry, inputs):
        block_queries, block_keys, block_values, decay_block = inputs
        running = jnp.cumsum(decay_block, axis=1)
        spread = running[:, :, None] - running[:, None, :]
        damping = jnp.exp(jnp.where(causal[None], spread, -jnp.inf))
        attention_scores = jnp.einsum(
            "xru,jru->rxj", block_queries, block_keys, preferred_element_type=jnp.float32
        )
        decay_weighted = (attention_scores * scale * damping).astype(jnp.bfloat16)
        inner_block_term = jnp.einsum(
            "svc,csj->vsj", decay_weighted, block_values, preferred_element_type=jnp.float32
        )
        carried = jnp.einsum(
            "nhd,hde->nhe",
            block_queries.astype(jnp.float32),
            carry,
            precision=lax.Precision.HIGHEST,
        )
        carried = carried * jnp.exp(running).T[:, :, None]
        decay_to_block_end = jnp.exp(running[:, -1:] - running).T[:, :, None] * scale
        state_update = jnp.einsum(
            "jok,jow->okw",
            block_keys.astype(jnp.float32) * decay_to_block_end,
            block_values.astype(jnp.float32),
            precision=lax.Precision.HIGHEST,
        )
        carry = carry * jnp.exp(running[:, -1])[:, None, None] + state_update
        return (carry, inner_block_term + carried)

    final, outputs = lax.scan(
        advance, state, (query_blocks, key_blocks, value_blocks, decay_blocks)
    )
    return (final, outputs.reshape(rows, heads, width))


def combine_states(earlier, later):
    return (earlier[0] * later[0], earlier[1] * later[0][:, None, None] + later[1])


def entering_state(totals, own_state):
    identity = (jnp.ones_like(totals), jnp.zeros_like(own_state))
    return entering((totals, own_state), "sp", combine_states, identity)[1]


def on_device(
    query_rows,
    key_rows,
    value_rows,
    gate_rows,
    log_decay,
    residual,
    head_gain,
    out_weight,
    norm_gain,
    expert_ids,
    route_weights,
    expert_gate,
    expert_up,
    expert_down,
    shared_gate,
    shared_up,
    shared_down,
):
    seq_rows, local_width = query_rows.shape
    heads = local_width // HEAD
    out_full, gate_full, up_full, down_full = (
        lax.all_gather(out_weight, "tp", axis=1, tiled=True),
        lax.all_gather(expert_gate, "tp", axis=1, tiled=True),
        lax.all_gather(expert_up, "tp", axis=1, tiled=True),
        lax.all_gather(expert_down, "tp", axis=1, tiled=True),
    )
    queries = query_rows.reshape(seq_rows, heads, HEAD)
    key_heads = key_rows.reshape(seq_rows, heads, HEAD)
    values = value_rows.reshape(seq_rows, heads, HEAD)
    zero_state = jnp.zeros((heads, HEAD, HEAD), jnp.float32)
    running = jnp.cumsum(log_decay, axis=1)
    totals = jnp.exp(running[:, -1])
    own_state, retained = block_pass(queries, key_heads, values, log_decay, zero_state)
    incoming = entering_state(totals, own_state)
    readout = jnp.einsum(
        "nhd,hde->nhe", queries.astype(jnp.float32), incoming, precision=lax.Precision.HIGHEST
    )
    retained = retained + readout * jnp.exp(running).T[:, :, None]
    centered = retained - jnp.mean(retained, axis=2, keepdims=True)
    normed = centered * lax.rsqrt(jnp.mean(centered * centered, axis=2, keepdims=True) + eps)
    ret_rows = (
        normed.reshape(seq_rows, local_width)
        * head_gain
        * jax.nn.silu(gate_rows.astype(jnp.float32))
    ).astype(jnp.bfloat16)
    token_rows = lax.all_to_all(ret_rows, "tp", split_axis=0, concat_axis=1, tiled=True)
    mixer = jnp.dot(token_rows, out_full, preferred_element_type=jnp.float32)
    hidden = (residual.astype(jnp.float32) + mixer).astype(jnp.bfloat16)
    hidden_wide = hidden.astype(jnp.float32)
    normed_rows = (
        hidden_wide
        * lax.rsqrt(jnp.mean(hidden_wide * hidden_wide, axis=1, keepdims=True) + eps)
        * norm_gain
    ).astype(jnp.bfloat16)
    shared_mid = (
        jax.nn.silu(jnp.dot(normed_rows, shared_gate, preferred_element_type=jnp.float32))
        * jnp.dot(normed_rows, shared_up, preferred_element_type=jnp.float32)
    ).astype(jnp.bfloat16)
    shared_out = lax.dot_general(
        shared_mid, shared_down, (((1,), (1,)), ((), ())), preferred_element_type=jnp.float32
    )
    specialist_networks = lax.axis_size("sp")
    token_count, chosen_count = expert_ids.shape
    model_width = normed_rows.shape[1]
    capacity = 3 * token_count * chosen_count // (2 * specialist_networks)
    flat_ids = expert_ids.reshape(-1)
    matches = (
        flat_ids[:, None] == jnp.arange(specialist_networks, dtype=jnp.int32)[None, :]
    ).astype(jnp.int32)
    position = jnp.sum((jnp.cumsum(matches, axis=0) - 1) * matches, axis=1)
    slot = flat_ids * capacity + position
    owner = jnp.arange(token_count * chosen_count, dtype=jnp.int32) // chosen_count
    slot_token = jnp.zeros((specialist_networks * capacity,), jnp.int32).at[slot].set(owner)
    slot_live = jnp.zeros((specialist_networks * capacity,), jnp.bfloat16).at[slot].set(1.0)
    outgoing = (normed_rows[slot_token] * slot_live[:, None]).reshape(
        specialist_networks, capacity, model_width
    )
    arrived = lax.all_to_all(outgoing, "sp", split_axis=0, concat_axis=0, tiled=True)
    flat_rows = arrived.reshape(-1, model_width)
    middle = (
        jax.nn.silu(jnp.dot(flat_rows, gate_full, preferred_element_type=jnp.float32))
        * jnp.dot(flat_rows, up_full, preferred_element_type=jnp.float32)
    ).astype(jnp.bfloat16)
    outcome = lax.dot_general(
        middle, down_full, (((1,), (1,)), ((), ())), preferred_element_type=jnp.float32
    ).astype(jnp.bfloat16)
    processed = outcome.reshape(arrived.shape)
    returned = lax.all_to_all(processed, "sp", split_axis=0, concat_axis=0, tiled=True)
    picked = returned.reshape(specialist_networks * capacity, model_width)[slot].astype(jnp.float32)
    decay_weighted = picked * route_weights.reshape(-1)[:, None]
    routed = jnp.sum(decay_weighted.reshape(token_count, chosen_count, model_width), axis=1)
    return (hidden_wide + routed + shared_out).astype(jnp.bfloat16)


def solution(mesh):
    placed = (
        P("sp", "tp"),
        P("sp", "tp"),
        P("sp", "tp"),
        P("sp", "tp"),
        P("tp", "sp"),
        P(("sp", "tp"), None),
        P("tp"),
        P(None, "tp"),
        P(),
        P(("sp", "tp"), None),
        P(("sp", "tp"), None),
        P(None, ("sp", "tp")),
        P(None, ("sp", "tp")),
        P(None, ("sp", "tp")),
        P(),
        P(),
        P(),
    )
    return jax.shard_map(
        on_device, mesh=mesh, in_specs=placed, out_specs=P(("sp", "tp"), None), check_vma=False
    )
```

profile of v0, /device:TPU:0, one launch (start us, length us, event | category | flops | bytes accessed | tf_op | source)
XLA Modules:
  0.0 303.6 jit_solution(6103581982348177756)
XLA Ops:
  11.2 2.4 reshape.235
  17.1 11.4 %all-reduce = f32[8]{0:T(128)S(1)} all-reduce(f32[8]{0:T(128)S(1)} %bitcast_dynamic-update-slice_fusion), channel_id=2, replica_groups=mesh['sp'=4,'tp'=8] {'sp'}, use_global_device_ids=true, to_apply=%add | all-reduce | flops 8 | bytes 64
  29.1 3.2 %reshape.233 = bf16[4,512,2,64]{3,2,1,0:T(2,128)(2,1)} reshape(bf16[2048,128]{1,0:T(8,128)(2,1)} %param.22) | data formatting | bytes 1048576 | tf_op jit(solution)/shard_map/reshape;reshape | solution.py:30
  32.3 3.5 %copy.66 = bf16[4,512,2,64]{1,3,2,0:T(8,128)(2,1)} copy(bf16[4,512,2,64]{3,2,1,0:T(2,128)(2,1)} %reshape.233) | data formatting | bytes 1048576
  35.8 3.2 %reshape.234 = bf16[4,512,2,64]{3,2,1,0:T(2,128)(2,1)} reshape(bf16[2048,128]{1,0:T(8,128)(2,1)} %param.23) | data formatting | bytes 1048576 | tf_op jit(solution)/shard_map/reshape;reshape | solution.py:31
  39.0 3.5 %copy.67 = bf16[4,512,2,64]{1,3,2,0:T(8,128)(2,1)} copy(bf16[4,512,2,64]{3,2,1,0:T(2,128)(2,1)} %reshape.234) | data formatting | bytes 1048576
  44.3 50.0 %while.27 = (s32[]{:T(128)}, f32[2,64,64]{2,1,0:T(8,128)S(1)}, f32[4,512,2,64]{1,0,3,2:T(4,128)}, f32[4,2,512]{2,1,0:T(2,128)S(1)}, bf16[4,512,2,64]{1,3,2,0:T(8...) while((s32[]{:T(128)}, f32[2,64,64]{2,1,0:T(8,128)S(1)}, ...), condition=%wide.region_3.4_spmd.clone, body=%wide.region_0.3_spmd.clone.sunk | while | flops 238192672 | bytes 3317096 | solution.py:65
  49.3 6.2 %dynamic_update_slice.6 = f32[4,512,2,64]{1,0,3,2:T(4,128)} dynamic-update-slice(f32[4,512,2,64]{1,0,3,2:T(4,128)} %get-tuple-element.330, f32[1,512,2,64]{1,0,3,2:T(1,128)S(1)} %copy.122, s32[]{:T(128)} %get-tuple-element.328, s32[]{:T(128)} %constant.94.clone.1..sunk, s32[]{:T(128)} %constant.94.clone.1..sunk, s32[]{:T(128)} %constant.94.clone.1..sunk) | dynamic-update-slice | bytes 524292 | tf_op jit(solution)/shard_map/while/body/jit(dynamic_update_index_in_dim)/dynamic_update_slice | solution.py:65
  61.9 6.2 %dynamic_update_slice.6 = f32[4,512,2,64]{1,0,3,2:T(4,128)} dynamic-update-slice(f32[4,512,2,64]{1,0,3,2:T(4,128)} %get-tuple-element.330, f32[1,512,2,64]{1,0,3,2:T(1,128)S(1)} %copy.122, s32[]{:T(128)} %get-tuple-element.328, s32[]{:T(128)} %constant.94.clone.1..sunk, s32[]{:T(128)} %constant.94.clone.1..sunk, s32[]{:T(128)} %constant.94.clone.1..sunk) | dynamic-update-slice | bytes 524292 | tf_op jit(solution)/shard_map/while/body/jit(dynamic_update_index_in_dim)/dynamic_update_slice | solution.py:65
  74.4 6.1 %dynamic_update_slice.6 = f32[4,512,2,64]{1,0,3,2:T(4,128)} dynamic-update-slice(f32[4,512,2,64]{1,0,3,2:T(4,128)} %get-tuple-element.330, f32[1,512,2,64]{1,0,3,2:T(1,128)S(1)} %copy.122, s32[]{:T(128)} %get-tuple-element.328, s32[]{:T(128)} %constant.94.clone.1..sunk, s32[]{:T(128)} %constant.94.clone.1..sunk, s32[]{:T(128)} %constant.94.clone.1..sunk) | dynamic-update-slice | bytes 524292 | tf_op jit(solution)/shard_map/while/body/jit(dynamic_update_index_in_dim)/dynamic_update_slice | solution.py:65
  86.9 6.1 %dynamic_update_slice.6 = f32[4,512,2,64]{1,0,3,2:T(4,128)} dynamic-update-slice(f32[4,512,2,64]{1,0,3,2:T(4,128)} %get-tuple-element.330, f32[1,512,2,64]{1,0,3,2:T(1,128)S(1)} %copy.122, s32[]{:T(128)} %get-tuple-element.328, s32[]{:T(128)} %constant.94.clone.1..sunk, s32[]{:T(128)} %constant.94.clone.1..sunk, s32[]{:T(128)} %constant.94.clone.1..sunk) | dynamic-update-slice | bytes 524292 | tf_op jit(solution)/shard_map/while/body/jit(dynamic_update_index_in_dim)/dynamic_update_slice | solution.py:65
  94.3 8.0 %all-gather.1 = f32[8,64,64]{2,1,0:T(8,128)S(1)} all-gather(f32[2,64,64]{2,1,0:T(8,128)S(1)} %get-tuple-element.143), channel_id=3, replica_groups=mesh['sp'=4,'tp'=8] {'sp'}, dimensions={0}, use_global_device_ids=true | all-gather | bytes 163840 | tf_op jit(solution)/shard_map/all_gather | solution.py:13
  102.3 2.3 while.28
  113.3 4.8 %all-to-all-start = ((bf16[8,256,128]{2,1,0:T(8,128)(2,1)}), bf16[8,256,128]{2,1,0:T(8,128)(2,1)S(1)}, u32[]{:S(2)}, u32[]{:S(2)}) async-start(bf16[8,256,128]{2,1,0:T(8,128)(2,1)} %bitcast.159), calls=%async_computation | async-start | bytes 1048576 | tf_op jit(solution)/shard_map/all_to_all | solution.py:126
  120.7 2.4 scatter_custom_fusion
  123.1 3.8 %scatter_custom_fusion.1 = bf16[768]{0:T(1024)(128)(2,1)S(1)} fusion(s32[512]{0:T(512)S(1)} %bitcast.173, bf16[512]{0:T(512)(128)(2,1)S(1)} %broadcast.147, bf16[]{:T(256)} %constant.106.clone.1), kind=kCustom, calls=%fused_computation.116 | custom fusion | bytes 1538 | tf_op jit(solution)/shard_map/scatter | solution.py:154
  127.0 20.6 %all-to-all-done = bf16[8,256,128]{2,1,0:T(8,128)(2,1)S(1)} async-done(((bf16[8,256,128]{2,1,0:T(8,128)(2,1)}), bf16[8,256,128]{2,1,0:T(8,128)(2,1)S(1)}, u32[]{:S(2)}, u32[]{:S(2)}) %all-to-all-start) | async-done | bytes 524320 | tf_op jit(solution)/shard_map/all_to_all | solution.py:126
  147.9 4.0 %fusion.46 = (f32[256]{0:T(256)S(1)}, bf16[256,2048]{1,0:T(8,128)(2,1)S(1)}) fusion(bf16[256,1024]{0,1:T(8,128)(2,1)S(1)} %bitcast.163, bf16[1024,2048]{1,0:T(8,128)(2,1)} %all-gather.7.cloned.1.call-done, bf16[256,2048]{1,0:T(8,128)(2,1)} %param.26), kind=kOutput, calls=%fused_computation.66 | convolution fusion | flops 1076887296 | bytes 6816768 | tf_op jit(solution)/shard_map/dot_general | solution.py:127
  153.2 4.3 %gather_fusion = bf16[768,2048]{1,0:T(8,128)(2,1)} fusion(bf16[256,2048]{1,0:T(8,128)(2,1)S(1)} %fusion.48, s32[1024]{0:T(1024)S(1)} %pad_clamp_fusion.1), kind=kCustom, calls=%fused_computation | custom fusion | bytes 6294528 | tf_op jit(solution)/shard_map/gather | solution.py:155
  157.5 3.8 %broadcast_multiply_fusion = bf16[4,192,2048]{2,1,0:T(8,128)(2,1)} fusion(bf16[4,192,2048]{2,1,0:T(8,128)(2,1)} %bitcast.156, bf16[4,192]{1,0:T(4,128)(2,1)S(1)} %mul.185), kind=kLoop, calls=%fused_computation.69 | loop fusion | flops 1572864 | bytes 6292992 | tf_op jit(solution)/shard_map/mul | solution.py:155
  161.3 4.7 %all-to-all-start.1 = ((bf16[4,192,2048]{2,1,0:T(8,128)(2,1)}), bf16[4,192,2048]{2,1,0:T(8,128)(2,1)}, u32[]{:S(2)}, u32[]{:S(2)}) async-start(bf16[4,192,2048]{2,1,0:T(8,128)(2,1)} %broadcast_multiply_fusion), calls=%async_computation.1 | async-start | bytes 6291456 | tf_op jit(solution)/shard_map/all_to_all | solution.py:158
  166.1 36.7 %all-to-all-done.1 = bf16[4,192,2048]{2,1,0:T(8,128)(2,1)} async-done(((bf16[4,192,2048]{2,1,0:T(8,128)(2,1)}), bf16[4,192,2048]{2,1,0:T(8,128)(2,1)}, u32[]{:S(2)}, u32[]{:S(2)}) %all-to-all-start.1) | async-done | bytes 3145760 | tf_op jit(solution)/shard_map/all_to_all | solution.py:158
  202.7 8.3 %fusion.78 = f32[768,1024]{1,0:T(8,128)} fusion(bf16[768,2048]{1,0:T(8,128)(2,1)} %bitcast.16, bf16[2048,1024]{1,0:T(8,128)(2,1)} %all-gather.9.cloned.1.call-done), kind=kOutput, calls=%fused_computation.125 | convolution fusion | flops 3221225472 | bytes 10485760 | tf_op jit(solution)/shard_map/dot_general | solution.py:161
  211.0 3.9 %all-gather.13.cloned.1.call-done = bf16[2048,1024]{1,0:T(8,128)(2,1)} async-done(((bf16[2048,128]{1,0:T(8,128)(2,1)}), bf16[2048,1024]{1,0:T(8,128)(2,1)}) %all-gather.13.cloned.1.call-update) | async-done | bytes 4194320 | tf_op jit(solution)/shard_map/all_gather | solution.py:105
  214.9 12.5 %convolution_convert_fusion = bf16[768,2048]{1,0:T(8,128)(2,1)} fusion(bf16[2048,1024]{1,0:T(8,128)(2,1)} %all-gather.13.cloned.1.call-done, f32[768,1024]{1,0:T(8,128)} %fusion.78, bf16[768,2048]{1,0:T(8,128)(2,1)} %bitcast.16, bf16[2048,1024]{1,0:T(8,128)(2,1)} %all-gather.11.cloned.1.call-done), kind=kOutput, calls=%fused_computation.54 | convolution fusion | flops 6448742400 | bytes 17825792 | tf_op jit(solution)/shard_map/dot_general | solution.py:164
  227.5 5.0 %all-to-all-start.2 = ((bf16[4,192,2048]{2,1,0:T(8,128)(2,1)}), bf16[4,192,2048]{2,1,0:T(8,128)(2,1)}, u32[]{:S(2)}, u32[]{:S(2)}) async-start(bf16[4,192,2048]{2,1,0:T(8,128)(2,1)} %bitcast.158), calls=%async_computation.2 | async-start | bytes 6291456 | tf_op jit(solution)/shard_map/all_to_all | solution.py:168
  232.7 3.2 %fusion.76 = f32[256,512]{1,0:T(8,128)} fusion(bf16[2048,512]{1,0:T(8,128)(2,1)} %param.35, bf16[256,2048]{1,0:T(8,128)(2,1)S(1)} %copy-done.2, f32[2048]{0:T(1024)S(1)} %copy-done.5, f32[256]{0:T(256)S(1)} %add_rsqrt_fusion.1), kind=kOutput, calls=%fused_computation.124 | convolution fusion | flops 538968064 | bytes 3679232 | tf_op jit(solution)/shard_map/dot_general | solution.py:136
  235.8 33.3 %all-to-all-done.2 = bf16[4,192,2048]{2,1,0:T(8,128)(2,1)} async-done(((bf16[4,192,2048]{2,1,0:T(8,128)(2,1)}), bf16[4,192,2048]{2,1,0:T(8,128)(2,1)}, u32[]{:S(2)}, u32[]{:S(2)}) %all-to-all-start.2) | async-done | bytes 3145760 | tf_op jit(solution)/shard_map/all_to_all | solution.py:168
  269.1 7.6 %gather_fusion.1 = bf16[512,2048]{1,0:T(8,128)(2,1)} fusion(bf16[768,2048]{1,0:T(8,128)(2,1)} %bitcast.18, s32[1024]{0:T(1024)S(1)} %pad_clamp_fusion), kind=kCustom, calls=%fused_computation.1 | custom fusion | bytes 4196352 | tf_op jit(solution)/shard_map/gather | solution.py:169
  276.7 5.4 %reshape.189 = f32[256,2,2048]{2,1,0:T(2,128)} reshape(bf16[512,2048]{1,0:T(8,128)(2,1)} %gather_fusion.1) | data formatting | bytes 6291456 | tf_op jit(solution)/shard_map/convert_element_type | solution.py:169
  282.1 10.1 %multiply_reduce_fusion = f32[256,2048]{1,0:T(8,128)} fusion(f32[256,2,2048]{2,1,0:T(2,128)} %reshape.189, f32[256,2]{1,0:T(8,128)S(1)} %copy.78), kind=kLoop, calls=%fused_computation.53 | loop fusion | flops 1572864 | bytes 6293504 | tf_op jit(solution)/shard_map/reduce_sum | solution.py:171
  292.3 4.8 %fusion.42 = bf16[256,2048]{1,0:T(8,128)(2,1)} fusion(bf16[2048,512]{1,0:T(8,128)(2,1)S(1)} %copy-done, f32[256,2048]{1,0:T(8,128)} %multiply_reduce_fusion, bf16[256,2048]{1,0:T(8,128)(2,1)S(1)} %copy-done.2, bf16[2048,512]{1,0:T(8,128)(2,1)} %param.36, f32[256,512]{1,0:T(8,128)} %fusion.76, f32[2048]{0:T(1024)S(1)} %copy-done.5, f32[256]{0:T(256)S(1)} %add_rsqrt_fusion.1), kind=kOutput, calls=%fused_computation.61 | convolution fusion | flops 1078722560 | bytes 8922112 | tf_op jit(solution)/shard_map/dot_general | solution.py:139
  (150 shorter events, 50.1 us)
Async XLA Ops:
  6.5 285.7 %copy-start = (bf16[2048,512]{1,0:T(8,128)(2,1)S(1)}, bf16[2048,512]{1,0:T(8,128)(2,1)}, u32[]{:S(2)}) copy-start(bf16[2048,512]{1,0:T(8,128)(2,1)} %param.37) | copy-start | bytes 6291460
  6.5 7.1 %copy-start.9 = (u32[32]{0:T(128)S(1)}, u32[32]{0:T(128)}, u32[]{:S(2)}) copy-start(u32[32]{0:T(128)} %constant.111) | copy-start | bytes 388
  6.5 2.8 copy-start.3
  6.5 141.3 %all-gather.7.cloned.1.call-start = ((), (), s32[]{:S(2)}) async-start(), calls=%async_computation.3 | async-start | bytes 4718592 | tf_op jit(solution)/shard_map/all_gather | solution.py:102
  7.3 158.8 %all-gather.9.cloned.1.call-start = ((), (), s32[]{:S(2)}) async-start(), calls=%async_computation.4 | async-start | bytes 4718592 | tf_op jit(solution)/shard_map/all_gather | solution.py:103
  8.0 203.0 %all-gather.11.cloned.1.call-start = ((), (), s32[]{:S(2)}) async-start(), calls=%async_computation.5 | async-start | bytes 4718592 | tf_op jit(solution)/shard_map/all_gather | solution.py:104
  8.7 206.2 %all-gather.13.cloned.1.call-start = ((), (), s32[]{:S(2)}) async-start(), calls=%async_computation.6 | async-start | bytes 4718592 | tf_op jit(solution)/shard_map/all_gather | solution.py:105
  94.3 12.3 %copy-start.4 = (f32[2048,2]{0,1:T(2,128)S(1)}, f32[2048,2]{0,1:T(2,128)}, u32[]{:S(2)}) copy-start(f32[2048,2]{0,1:T(2,128)} %exponential_bitcast_fusion.1) | copy-start | bytes 49156
  108.5 2.7 copy-start.8
  111.2 7.0 %copy-start.6 = (s32[256,2]{0,1:T(2,128)S(1)}, s32[256,2]{0,1:T(2,128)}, u32[]{:S(2)}) copy-start(s32[256,2]{0,1:T(2,128)} %param.30) | copy-start | bytes 6148
  113.3 34.3 %all-to-all-start = ((bf16[8,256,128]{2,1,0:T(8,128)(2,1)}), bf16[8,256,128]{2,1,0:T(8,128)(2,1)S(1)}, u32[]{:S(2)}, u32[]{:S(2)}) async-start(bf16[8,256,128]{2,1,0:T(8,128)(2,1)} %bitcast.159), calls=%async_computation | async-start | bytes 1048576 | tf_op jit(solution)/shard_map/all_to_all | solution.py:126
  147.9 5.0 %copy-start.5 = (f32[2048]{0:T(1024)S(1)}, f32[2048]{0:T(1024)}, u32[]{:S(2)}) copy-start(f32[2048]{0:T(1024)} %param.29) | copy-start | bytes 24580
  151.9 1.0 copy-start.1
  161.3 41.4 %all-to-all-start.1 = ((bf16[4,192,2048]{2,1,0:T(8,128)(2,1)}), bf16[4,192,2048]{2,1,0:T(8,128)(2,1)}, u32[]{:S(2)}, u32[]{:S(2)}) async-start(bf16[4,192,2048]{2,1,0:T(8,128)(2,1)} %broadcast_multiply_fusion), calls=%async_computation.1 | async-start | bytes 6291456 | tf_op jit(solution)/shard_map/all_to_all | solution.py:158
  227.5 5.0 %copy-start.7 = (f32[256,2]{0,1:T(2,128)S(1)}, f32[256,2]{0,1:T(2,128)}, u32[]{:S(2)}) copy-start(f32[256,2]{0,1:T(2,128)} %param.31) | copy-start | bytes 6148
  227.5 5.2 %copy-start.2 = (bf16[256,2048]{1,0:T(8,128)(2,1)S(1)}, bf16[256,2048]{1,0:T(8,128)(2,1)}, u32[]{:S(2)}) copy-start(bf16[256,2048]{1,0:T(8,128)(2,1)} %copy-done.1) | copy-start | bytes 3145732
  227.5 41.6 %all-to-all-start.2 = ((bf16[4,192,2048]{2,1,0:T(8,128)(2,1)}), bf16[4,192,2048]{2,1,0:T(8,128)(2,1)}, u32[]{:S(2)}, u32[]{:S(2)}) async-start(bf16[4,192,2048]{2,1,0:T(8,128)(2,1)} %bitcast.158), calls=%async_computation.2 | async-start | bytes 6291456 | tf_op jit(solution)/shard_map/all_to_all | solution.py:168
Sparse Core Ops, SparseCore 0:
  8.9 50.5 all-gather.6
  61.1 45.9 all-gather.8
  108.8 58.4 all-gather.10
  168.7 46.2 all-gather.12
where the time goes:
time: 305 us; the launch traced here: 304 us
  waiting for transfers between devices  97.1 us (32%)
  local copies, waits for them, and re-layouts  80.6 us (26%)
  matrix products  53 us (17%)
  other arithmetic  24.5 us (8%)
  blocking collectives  19.4 us (6%)
  starting transfers between devices  14.6 us (5%)
  between operations  14.1 us (5%)
    all_to_all x1, waiting for transfers between devices, on_device(): lax.all_to_all(outgoing, 'sp', split_axis=0, concat_axis=0, tiled=True)  36.7 us
    all_to_all x1, waiting for transfers between devices, on_device(): lax.all_to_all(processed, 'sp', split_axis=0, concat_axis=0, tiled=True)  33.3 us
    dynamic_update_slice x8, local copies, waits for them, and re-layouts, block_pass(): lax.scan(advance, state, (query_blocks, key_blocks, value_blocks, decay_b...  25.7 us
    all_to_all x1, waiting for transfers between devices, on_device(): lax.all_to_all(ret_rows, 'tp', split_axis=0, concat_axis=1, tiled=True)  20.6 us
    unnamed x32, local copies, waits for them, and re-layouts  13 us
    dot_general x1, matrix products, on_device(): lax.dot_general(middle, down_full, (((1,), (1,)), ((), ())), preferred_el...  12.5 us
    unnamed x1, blocking collectives  11.4 us
    reduce_sum x1, other arithmetic, on_device(): jnp.sum(decay_weighted.reshape(token_count, chosen_count, model_width), a...  10.1 us
  transfers between devices with their start and end apart: 7, of which 4 were waited for; matrix products, arithmetic and copies ran while one was open for 38% of the time, Pallas kernels for 0%

commit v1 on v0

--- a/solution.py
+++ b/solution.py
@@ -123,7 +123,18 @@
         * head_gain
         * jax.nn.silu(gate_rows.astype(jnp.float32))
     ).astype(jnp.bfloat16)
-    token_rows = lax.all_to_all(ret_rows, "tp", split_axis=0, concat_axis=1, tiled=True)
+
+    def pass_spot(field, d0, dimension_no):
+        part_next = lax.all_to_all(
+            jnp.stack(jnp.split(field, lax.axis_size("tp"), axis=d0)),
+            axis_name="tp",
+            split_axis=0,
+            concat_axis=0,
+        )
+        now = jnp.concatenate(part_next, axis=dimension_no)
+        return now
+
+    token_rows = pass_spot(ret_rows, 0, 1)
     mixer = jnp.dot(token_rows, out_full, preferred_element_type=jnp.float32)
     hidden = (residual.astype(jnp.float32) + mixer).astype(jnp.bfloat16)
     hidden_wide = hidden.astype(jnp.float32)

time: 305 us -> 305 us (level)
  local copies, waits for them, and re-layouts: 80.6 us -> 86 us
  waiting for transfers between devices: 97.1 us -> 92.8 us
    unnamed x32 -> x40, local copies, waits for them, and re-layouts: 13 us -> 19.5 us
  transfers between devices with their start and end apart: 7 -> 7, of which waited for: 4 -> 4; matrix products, arithmetic and copies ran while one was open for 38% -> 40% of each run, Pallas kernels for 0% -> 0%
where the time goes in v1:
time: 305 us; the launch traced here: 303 us
  waiting for transfers between devices  92.8 us (30%)
  local copies, waits for them, and re-layouts  86 us (28%)
  matrix products  52.8 us (17%)
  other arithmetic  23 us (8%)
  blocking collectives  19.4 us (6%)
  starting transfers between devices  14.6 us (5%)
  between operations  14.1 us (5%)
    all_to_all x1, waiting for transfers between devices, on_device(): lax.all_to_all(outgoing, 'sp', split_axis=0, concat_axis=0, tiled=True)  36.1 us
    all_to_all x1, waiting for transfers between devices, on_device(): lax.all_to_all(processed, 'sp', split_axis=0, concat_axis=0, tiled=True)  33.3 us
    dynamic_update_slice x8, local copies, waits for them, and re-layouts, block_pass(): lax.scan(advance, state, (query_blocks, key_blocks, value_blocks, decay_b...  25.7 us
    unnamed x40, local copies, waits for them, and re-layouts  19.5 us
    all_to_all x1, waiting for transfers between devices, pass_spot(): lax.all_to_all(jnp.stack(jnp.split(field, lax.axis_size('tp'), axis=d0)),...  18.3 us
    dot_general x1, matrix products, on_device(): lax.dot_general(middle, down_full, (((1,), (1,)), ((), ())), preferred_el...  12.5 us
    unnamed x1, blocking collectives  11.4 us
    reduce_sum x1, other arithmetic, on_device(): jnp.sum(decay_weighted.reshape(token_count, chosen_count, model_width), a...  10.1 us
  transfers between devices with their start and end apart: 7, of which 4 were waited for; matrix products, arithmetic and copies ran while one was open for 40% of the time, Pallas kernels for 0%

profile of v1, /device:TPU:0, one launch (start us, length us, event | category | flops | bytes accessed | tf_op | source)
XLA Modules:
  0.0 302.9 jit_solution(1000893558062869301)
XLA Ops:
  11.2 2.4 reshape.240
  17.1 11.4 %all-reduce = f32[8]{0:T(128)S(1)} all-reduce(f32[8]{0:T(128)S(1)} %bitcast_dynamic-update-slice_fusion), channel_id=2, replica_groups=mesh['sp'=4,'tp'=8] {'sp'}, use_global_device_ids=true, to_apply=%add | all-reduce | flops 8 | bytes 64
  29.1 3.2 %reshape.238 = bf16[4,512,2,64]{3,2,1,0:T(2,128)(2,1)} reshape(bf16[2048,128]{1,0:T(8,128)(2,1)} %param.22) | data formatting | bytes 1048576 | tf_op jit(solution)/shard_map/reshape;reshape | solution.py:30
  32.3 3.5 %copy.48 = bf16[4,512,2,64]{1,3,2,0:T(8,128)(2,1)} copy(bf16[4,512,2,64]{3,2,1,0:T(2,128)(2,1)} %reshape.238) | data formatting | bytes 1048576
  35.8 3.2 %reshape.239 = bf16[4,512,2,64]{3,2,1,0:T(2,128)(2,1)} reshape(bf16[2048,128]{1,0:T(8,128)(2,1)} %param.23) | data formatting | bytes 1048576 | tf_op jit(solution)/shard_map/reshape;reshape | solution.py:31
  39.0 3.5 %copy.49 = bf16[4,512,2,64]{1,3,2,0:T(8,128)(2,1)} copy(bf16[4,512,2,64]{3,2,1,0:T(2,128)(2,1)} %reshape.239) | data formatting | bytes 1048576
  44.3 50.0 %while.27 = (s32[]{:T(128)}, f32[2,64,64]{2,1,0:T(8,128)S(1)}, f32[4,512,2,64]{1,0,3,2:T(4,128)}, f32[4,2,512]{2,1,0:T(2,128)S(1)}, bf16[4,512,2,64]{1,3,2,0:T(8...) while((s32[]{:T(128)}, f32[2,64,64]{2,1,0:T(8,128)S(1)}, ...), condition=%wide.region_3.4_spmd.clone, body=%wide.region_0.3_spmd.clone.sunk | while | flops 238192672 | bytes 3317096 | solution.py:65
  49.3 6.2 %dynamic_update_slice.6 = f32[4,512,2,64]{1,0,3,2:T(4,128)} dynamic-update-slice(f32[4,512,2,64]{1,0,3,2:T(4,128)} %get-tuple-element.323, f32[1,512,2,64]{1,0,3,2:T(1,128)S(1)} %copy.103, s32[]{:T(128)} %get-tuple-element.321, s32[]{:T(128)} %constant.94.clone.1..sunk, s32[]{:T(128)} %constant.94.clone.1..sunk, s32[]{:T(128)} %constant.94.clone.1..sunk) | dynamic-update-slice | bytes 524292 | tf_op jit(solution)/shard_map/while/body/jit(dynamic_update_index_in_dim)/dynamic_update_slice | solution.py:65
  61.9 6.2 %dynamic_update_slice.6 = f32[4,512,2,64]{1,0,3,2:T(4,128)} dynamic-update-slice(f32[4,512,2,64]{1,0,3,2:T(4,128)} %get-tuple-element.323, f32[1,512,2,64]{1,0,3,2:T(1,128)S(1)} %copy.103, s32[]{:T(128)} %get-tuple-element.321, s32[]{:T(128)} %constant.94.clone.1..sunk, s32[]{:T(128)} %constant.94.clone.1..sunk, s32[]{:T(128)} %constant.94.clone.1..sunk) | dynamic-update-slice | bytes 524292 | tf_op jit(solution)/shard_map/while/body/jit(dynamic_update_index_in_dim)/dynamic_update_slice | solution.py:65
  74.4 6.1 %dynamic_update_slice.6 = f32[4,512,2,64]{1,0,3,2:T(4,128)} dynamic-update-slice(f32[4,512,2,64]{1,0,3,2:T(4,128)} %get-tuple-element.323, f32[1,512,2,64]{1,0,3,2:T(1,128)S(1)} %copy.103, s32[]{:T(128)} %get-tuple-element.321, s32[]{:T(128)} %constant.94.clone.1..sunk, s32[]{:T(128)} %constant.94.clone.1..sunk, s32[]{:T(128)} %constant.94.clone.1..sunk) | dynamic-update-slice | bytes 524292 | tf_op jit(solution)/shard_map/while/body/jit(dynamic_update_index_in_dim)/dynamic_update_slice | solution.py:65
  86.9 6.1 %dynamic_update_slice.6 = f32[4,512,2,64]{1,0,3,2:T(4,128)} dynamic-update-slice(f32[4,512,2,64]{1,0,3,2:T(4,128)} %get-tuple-element.323, f32[1,512,2,64]{1,0,3,2:T(1,128)S(1)} %copy.103, s32[]{:T(128)} %get-tuple-element.321, s32[]{:T(128)} %constant.94.clone.1..sunk, s32[]{:T(128)} %constant.94.clone.1..sunk, s32[]{:T(128)} %constant.94.clone.1..sunk) | dynamic-update-slice | bytes 524292 | tf_op jit(solution)/shard_map/while/body/jit(dynamic_update_index_in_dim)/dynamic_update_slice | solution.py:65
  94.3 8.0 %all-gather.1 = f32[8,64,64]{2,1,0:T(8,128)S(1)} all-gather(f32[2,64,64]{2,1,0:T(8,128)S(1)} %get-tuple-element.143), channel_id=3, replica_groups=mesh['sp'=4,'tp'=8] {'sp'}, dimensions={0}, use_global_device_ids=true | all-gather | bytes 163840 | tf_op jit(solution)/shard_map/all_gather | solution.py:13
  102.3 2.3 while.28
  117.2 4.8 %all-to-all-start = ((bf16[8,256,128]{1,2,0:T(8,128)(2,1)}), bf16[8,256,128]{1,2,0:T(8,128)(2,1)S(1)}, u32[]{:S(2)}, u32[]{:S(2)}) async-start(bf16[8,256,128]{1,2,0:T(8,128)(2,1)} %fusion.61), calls=%async_computation | async-start | bytes 1048576 | tf_op jit(solution)/shard_map/all_to_all | solution.py:128
  124.6 2.4 scatter_custom_fusion
  127.0 3.8 %scatter_custom_fusion.1 = bf16[768]{0:T(1024)(128)(2,1)S(1)} fusion(s32[512]{0:T(512)S(1)} %bitcast.207, bf16[512]{0:T(512)(128)(2,1)S(1)} %broadcast.147, bf16[]{:T(256)} %constant.106.clone.1), kind=kCustom, calls=%fused_computation.133 | custom fusion | bytes 1538 | tf_op jit(solution)/shard_map/scatter | solution.py:165
  130.9 18.3 %all-to-all-done = bf16[8,256,128]{1,2,0:T(8,128)(2,1)S(1)} async-done(((bf16[8,256,128]{1,2,0:T(8,128)(2,1)}), bf16[8,256,128]{1,2,0:T(8,128)(2,1)S(1)}, u32[]{:S(2)}, u32[]{:S(2)}) %all-to-all-start) | async-done | bytes 524320 | tf_op jit(solution)/shard_map/all_to_all | solution.py:128
  149.2 3.9 %fusion.46 = (f32[256]{0:T(256)S(1)}, bf16[256,2048]{1,0:T(8,128)(2,1)S(1)}) fusion(bf16[256,1024]{0,1:T(8,128)(2,1)S(1)} %bitcast.197, bf16[1024,2048]{1,0:T(8,128)(2,1)} %all-gather.7.cloned.1.call-done, bf16[256,2048]{1,0:T(8,128)(2,1)} %param.26), kind=kOutput, calls=%fused_computation.66 | convolution fusion | flops 1076887296 | bytes 6816768 | tf_op jit(solution)/shard_map/dot_general | solution.py:138
  154.4 4.3 %gather_fusion = bf16[768,2048]{1,0:T(8,128)(2,1)} fusion(bf16[256,2048]{1,0:T(8,128)(2,1)S(1)} %fusion.48, s32[1024]{0:T(1024)S(1)} %pad_clamp_fusion.1), kind=kCustom, calls=%fused_computation | custom fusion | bytes 6294528 | tf_op jit(solution)/shard_map/gather | solution.py:166
  158.7 4.0 %broadcast_multiply_fusion = bf16[4,192,2048]{2,1,0:T(8,128)(2,1)} fusion(bf16[4,192,2048]{2,1,0:T(8,128)(2,1)} %bitcast.193, bf16[4,192]{1,0:T(4,128)(2,1)S(1)} %mul.185), kind=kLoop, calls=%fused_computation.69 | loop fusion | flops 1572864 | bytes 6292992 | tf_op jit(solution)/shard_map/mul | solution.py:166
  162.7 4.7 %all-to-all-start.1 = ((bf16[4,192,2048]{2,1,0:T(8,128)(2,1)}), bf16[4,192,2048]{2,1,0:T(8,128)(2,1)}, u32[]{:S(2)}, u32[]{:S(2)}) async-start(bf16[4,192,2048]{2,1,0:T(8,128)(2,1)} %broadcast_multiply_fusion), calls=%async_computation.1 | async-start | bytes 6291456 | tf_op jit(solution)/shard_map/all_to_all | solution.py:169
  167.4 36.1 %all-to-all-done.1 = bf16[4,192,2048]{2,1,0:T(8,128)(2,1)} async-done(((bf16[4,192,2048]{2,1,0:T(8,128)(2,1)}), bf16[4,192,2048]{2,1,0:T(8,128)(2,1)}, u32[]{:S(2)}, u32[]{:S(2)}) %all-to-all-start.1) | async-done | bytes 3145760 | tf_op jit(solution)/shard_map/all_to_all | solution.py:169
  203.6 8.2 %fusion.86 = f32[768,1024]{1,0:T(8,128)} fusion(bf16[768,2048]{1,0:T(8,128)(2,1)} %bitcast.23, bf16[2048,1024]{1,0:T(8,128)(2,1)} %all-gather.9.cloned.1.call-done), kind=kOutput, calls=%fused_computation.142 | convolution fusion | flops 3221225472 | bytes 10485760 | tf_op jit(solution)/shard_map/dot_general | solution.py:172
  211.8 2.5 all-gather.13.cloned.1.call-done
  214.3 12.5 %convolution_convert_fusion = bf16[768,2048]{1,0:T(8,128)(2,1)} fusion(bf16[2048,1024]{1,0:T(8,128)(2,1)} %all-gather.13.cloned.1.call-done, f32[768,1024]{1,0:T(8,128)} %fusion.86, bf16[768,2048]{1,0:T(8,128)(2,1)} %bitcast.23, bf16[2048,1024]{1,0:T(8,128)(2,1)} %all-gather.11.cloned.1.call-done), kind=kOutput, calls=%fused_computation.54 | convolution fusion | flops 6448742400 | bytes 17825792 | tf_op jit(solution)/shard_map/dot_general | solution.py:175
  226.8 5.0 %all-to-all-start.2 = ((bf16[4,192,2048]{2,1,0:T(8,128)(2,1)}), bf16[4,192,2048]{2,1,0:T(8,128)(2,1)}, u32[]{:S(2)}, u32[]{:S(2)}) async-start(bf16[4,192,2048]{2,1,0:T(8,128)(2,1)} %bitcast.194), calls=%async_computation.2 | async-start | bytes 6291456 | tf_op jit(solution)/shard_map/all_to_all | solution.py:179
  232.0 3.2 %fusion.84 = f32[256,512]{1,0:T(8,128)} fusion(bf16[2048,512]{1,0:T(8,128)(2,1)} %param.35, bf16[256,2048]{1,0:T(8,128)(2,1)S(1)} %copy-done.2, f32[2048]{0:T(1024)S(1)} %copy-done.5, f32[256]{0:T(256)S(1)} %add_rsqrt_fusion.1), kind=kOutput, calls=%fused_computation.141 | convolution fusion | flops 538968064 | bytes 3679232 | tf_op jit(solution)/shard_map/dot_general | solution.py:147
  235.1 33.3 %all-to-all-done.2 = bf16[4,192,2048]{2,1,0:T(8,128)(2,1)} async-done(((bf16[4,192,2048]{2,1,0:T(8,128)(2,1)}), bf16[4,192,2048]{2,1,0:T(8,128)(2,1)}, u32[]{:S(2)}, u32[]{:S(2)}) %all-to-all-start.2) | async-done | bytes 3145760 | tf_op jit(solution)/shard_map/all_to_all | solution.py:179
  268.5 7.6 %gather_fusion.1 = bf16[512,2048]{1,0:T(8,128)(2,1)} fusion(bf16[768,2048]{1,0:T(8,128)(2,1)} %bitcast.25, s32[1024]{0:T(1024)S(1)} %pad_clamp_fusion), kind=kCustom, calls=%fused_computation.1 | custom fusion | bytes 4196352 | tf_op jit(solution)/shard_map/gather | solution.py:180
  276.0 5.4 %reshape.194 = f32[256,2,2048]{2,1,0:T(2,128)} reshape(bf16[512,2048]{1,0:T(8,128)(2,1)} %gather_fusion.1) | data formatting | bytes 6291456 | tf_op jit(solution)/shard_map/convert_element_type | solution.py:180
  281.5 10.1 %multiply_reduce_fusion = f32[256,2048]{1,0:T(8,128)} fusion(f32[256,2,2048]{2,1,0:T(2,128)} %reshape.194, f32[256,2]{1,0:T(8,128)S(1)} %copy.59), kind=kLoop, calls=%fused_computation.53 | loop fusion | flops 1572864 | bytes 6293504 | tf_op jit(solution)/shard_map/reduce_sum | solution.py:182
  291.6 4.8 %fusion.42 = bf16[256,2048]{1,0:T(8,128)(2,1)} fusion(bf16[2048,512]{1,0:T(8,128)(2,1)S(1)} %copy-done, f32[256,2048]{1,0:T(8,128)} %multiply_reduce_fusion, bf16[256,2048]{1,0:T(8,128)(2,1)S(1)} %copy-done.2, bf16[2048,512]{1,0:T(8,128)(2,1)} %param.36, f32[256,512]{1,0:T(8,128)} %fusion.84, f32[2048]{0:T(1024)S(1)} %copy-done.5, f32[256]{0:T(256)S(1)} %add_rsqrt_fusion.1), kind=kOutput, calls=%fused_computation.61 | convolution fusion | flops 1078722560 | bytes 8922112 | tf_op jit(solution)/shard_map/dot_general | solution.py:150
  (157 shorter events, 53.7 us)
Async XLA Ops:
  6.5 285.0 %copy-start = (bf16[2048,512]{1,0:T(8,128)(2,1)S(1)}, bf16[2048,512]{1,0:T(8,128)(2,1)}, u32[]{:S(2)}) copy-start(bf16[2048,512]{1,0:T(8,128)(2,1)} %param.37) | copy-start | bytes 6291460
  6.5 7.1 %copy-start.9 = (u32[32]{0:T(128)S(1)}, u32[32]{0:T(128)}, u32[]{:S(2)}) copy-start(u32[32]{0:T(128)} %constant.111) | copy-start | bytes 388
  6.5 2.8 copy-start.3
  6.5 142.6 %all-gather.7.cloned.1.call-start = ((), (), s32[]{:S(2)}) async-start(), calls=%async_computation.3 | async-start | bytes 4718592 | tf_op jit(solution)/shard_map/all_gather | solution.py:102
  7.3 160.2 %all-gather.9.cloned.1.call-start = ((), (), s32[]{:S(2)}) async-start(), calls=%async_computation.4 | async-start | bytes 4718592 | tf_op jit(solution)/shard_map/all_gather | solution.py:103
  8.0 203.8 %all-gather.11.cloned.1.call-start = ((), (), s32[]{:S(2)}) async-start(), calls=%async_computation.5 | async-start | bytes 4718592 | tf_op jit(solution)/shard_map/all_gather | solution.py:104
  8.7 205.5 %all-gather.13.cloned.1.call-start = ((), (), s32[]{:S(2)}) async-start(), calls=%async_computation.6 | async-start | bytes 4718592 | tf_op jit(solution)/shard_map/all_gather | solution.py:105
  94.3 12.3 %copy-start.4 = (f32[2048,2]{0,1:T(2,128)S(1)}, f32[2048,2]{0,1:T(2,128)}, u32[]{:S(2)}) copy-start(f32[2048,2]{0,1:T(2,128)} %exponential_bitcast_fusion.1) | copy-start | bytes 49156
  108.3 2.4 copy-start.8
  110.7 11.4 %copy-start.6 = (s32[256,2]{0,1:T(2,128)S(1)}, s32[256,2]{0,1:T(2,128)}, u32[]{:S(2)}) copy-start(s32[256,2]{0,1:T(2,128)} %param.30) | copy-start | bytes 6148
  117.2 31.9 %all-to-all-start = ((bf16[8,256,128]{1,2,0:T(8,128)(2,1)}), bf16[8,256,128]{1,2,0:T(8,128)(2,1)S(1)}, u32[]{:S(2)}, u32[]{:S(2)}) async-start(bf16[8,256,128]{1,2,0:T(8,128)(2,1)} %fusion.61), calls=%async_computation | async-start | bytes 1048576 | tf_op jit(solution)/shard_map/all_to_all | solution.py:128
  149.2 4.9 %copy-start.5 = (f32[2048]{0:T(1024)S(1)}, f32[2048]{0:T(1024)}, u32[]{:S(2)}) copy-start(f32[2048]{0:T(1024)} %param.29) | copy-start | bytes 24580
  153.1 1.0 copy-start.1
  162.7 40.9 %all-to-all-start.1 = ((bf16[4,192,2048]{2,1,0:T(8,128)(2,1)}), bf16[4,192,2048]{2,1,0:T(8,128)(2,1)}, u32[]{:S(2)}, u32[]{:S(2)}) async-start(bf16[4,192,2048]{2,1,0:T(8,128)(2,1)} %broadcast_multiply_fusion), calls=%async_computation.1 | async-start | bytes 6291456 | tf_op jit(solution)/shard_map/all_to_all | solution.py:169
  226.8 5.0 %copy-start.7 = (f32[256,2]{0,1:T(2,128)S(1)}, f32[256,2]{0,1:T(2,128)}, u32[]{:S(2)}) copy-start(f32[256,2]{0,1:T(2,128)} %param.31) | copy-start | bytes 6148
  226.8 5.2 %copy-start.2 = (bf16[256,2048]{1,0:T(8,128)(2,1)S(1)}, bf16[256,2048]{1,0:T(8,128)(2,1)}, u32[]{:S(2)}) copy-start(bf16[256,2048]{1,0:T(8,128)(2,1)} %copy-done.1) | copy-start | bytes 3145732
  226.8 41.6 %all-to-all-start.2 = ((bf16[4,192,2048]{2,1,0:T(8,128)(2,1)}), bf16[4,192,2048]{2,1,0:T(8,128)(2,1)}, u32[]{:S(2)}, u32[]{:S(2)}) async-start(bf16[4,192,2048]{2,1,0:T(8,128)(2,1)} %bitcast.194), calls=%async_computation.2 | async-start | bytes 6291456 | tf_op jit(solution)/shard_map/all_to_all | solution.py:179
Sparse Core Ops, SparseCore 0:
  8.9 50.5 all-gather.6
  61.1 45.9 all-gather.8
  108.8 56.5 all-gather.10
  166.8 47.3 all-gather.12
